TPU v7x, 32 devices: a whole 2x2x4 slice. The times are simulated.
32 devices in a mesh: ep: 8 (over z, x), tp: 4 (over y, core).
Axes of the slice: x: 2, y: 2, z: 4, core: 2. Of those that a mesh axis runs over, the one named last changes fastest.
Arguments:
- tokens: bfloat16 [128, 4096], P('ep'), may hold values from -6 to 6
- norm_gain: float32 [4096], replicated, may hold values from 0.1 to 1.9
- query_weight: bfloat16 [4096, 2048], P('ep', 'tp'), may hold values from -0.09375 to 0.09375
- key_weight: bfloat16 [4096, 256], P('ep', 'tp'), may hold values from -0.09375 to 0.09375
- value_weight: bfloat16 [4096, 256], P('ep', 'tp'), may hold values from -0.09375 to 0.09375
- forget_weight: bfloat16 [4096, 32], P('ep', 'tp'), may hold values from -0.09375 to 0.09375
- forget_bias: float32 [32], P('tp'), may hold values from -1 to 2
- kv_cache: bfloat16 [128, 1024, 4, 128], P('ep', None, 'tp'), may hold values from -256 to 256, as said below
- log_gates: float32 [128, 1024, 32], P('ep', None, 'tp'), may hold values from -258 to 0
- lengths: int32 [128], P('ep'), may hold values from 128 to 1024, as said below
- out_weight: bfloat16 [2048, 4096], P('tp', 'ep'), may hold values from -0.125 to 0.125
- mix_gain: float32 [4096], replicated, may hold values from 0.1 to 1.9
- expert_gate: bfloat16 [8, 4096, 1024], P('ep', None, 'tp'), may hold values from -0.09375 to 0.09375
- expert_up: bfloat16 [8, 4096, 1024], P('ep', None, 'tp'), may hold values from -0.09375 to 0.09375
- expert_down: bfloat16 [8, 1024, 4096], P('ep', 'tp'), may hold values from -0.1875 to 0.1875
- routes: int32 [128, 4], P('ep'), may hold values from 0 to 7, all different within a row; in each aligned block of 16 rows (0 to 15, 16 to 31, ...) at most 16 rows name the same one
- route_weights: float32 [128, 4], P('ep'), may hold values from 0.2 to 1
- dense_gate: bfloat16 [4096, 4096], P(None, 'ep'), may hold values from -0.09375 to 0.09375
- dense_up: bfloat16 [4096, 4096], P(None, 'ep'), may hold values from -0.09375 to 0.09375
- dense_down: bfloat16 [4096, 4096], P('ep', 'tp'), may hold values from -0.09375 to 0.09375
- gate_vector: float32 [4096], replicated, may hold values from -0.09375 to 0.09375
Outputs:
- layer_out: bfloat16 [128, 4096], P('ep', 'tp')
Inputs may be any that keep to these rules, and one draw needn't show every extreme that they name: `kv_cache`: keys and values of the cached positions. `lengths`: some sequence uses all 1024 cached positions in every draw. A sequence's 4 experts differ. Among the routes of the 16 sequences of one index of ep no expert appears more than 16 times, and in every draw some expert appears exactly 16 times there; every expert is chosen somewhere.
All inputs are finite; a program needn't handle non-finite values.
Results may differ from a plain program's by a relative error of at most 0.012.
The roundings to bfloat16 on the way count: a program that leaves them out, or rounds other values in their place, can miss the bound.
Values may be sent and summed in bfloat16 or wider, within the bound.
No kernel may reach another device: no remote copies, remote signals or barrier semaphores. Data moves between devices by JAX's collectives and lax.ppermute only.
A program may use at most 128 MiB of HBM per device.

v0:
```python
import jax
import jax.numpy as jnp
from jax import lax
from jax.sharding import PartitionSpec as P

EPS = 1e-06


def rms_scaled(matrix, gains):
    values = matrix.astype(jnp.float32)
    return values * lax.rsqrt(jnp.mean(values * values, axis=-1, keepdims=True) + EPS) * gains


def attend_local(queries, key_new, value_new, forget, kv_cache, log_gates, lengths):
    seqs_here, cache_len, kv_count, double_width = kv_cache.shape
    head_width = double_width // 2
    group_size = queries.shape[1] // (kv_count * head_width)
    queries = queries.reshape(seqs_here, kv_count, group_size, head_width)
    key_new = key_new.reshape(seqs_here, kv_count, head_width)
    value_new = value_new.reshape(seqs_here, kv_count, head_width)
    cached_keys = kv_cache[..., :head_width]
    cached_values = kv_cache[..., head_width:]
    score_scale = head_width ** (-0.5)
    current_position = jnp.arange(cache_len, dtype=jnp.int32)
    is_last = (current_position[None, :] == lengths[:, None] - 1)[:, :, None]
    last_gate = jnp.sum(jnp.where(is_last, log_gates, 0.0), axis=1)
    newest = last_gate + forget
    gate_bias = newest[:, None, :] - log_gates
    gate_bias = gate_bias.reshape(seqs_here, cache_len, kv_count, group_size).transpose(0, 2, 3, 1)
    past_scores = (
        jnp.einsum("skgd,slkd->skgl", queries, cached_keys, preferred_element_type=jnp.float32)
        * score_scale
        + gate_bias
    )
    is_valid = (current_position[None, :] < lengths[:, None])[:, None, None, :]
    past_scores = jnp.where(is_valid, past_scores, -jnp.inf)
    own_score = (
        jnp.einsum("skgd,skd->skg", queries, key_new, preferred_element_type=jnp.float32)
        * score_scale
    )
    highest = jnp.maximum(jnp.max(past_scores, axis=-1), own_score)
    past_exp = jnp.exp(past_scores - highest[..., None])
    own_exp = jnp.exp(own_score - highest)
    totals = jnp.sum(past_exp, axis=-1) + own_exp
    past_weights = (past_exp / totals[..., None]).astype(jnp.bfloat16)
    own_weights = (own_exp / totals).astype(jnp.bfloat16)
    mixed_values = jnp.einsum(
        "skgl,slkd->skgd", past_weights, cached_values, preferred_element_type=jnp.float32
    )
    mixed_values = (
        mixed_values
        + own_weights.astype(jnp.float32)[..., None] * value_new.astype(jnp.float32)[:, :, None, :]
    )
    return mixed_values.astype(jnp.bfloat16).reshape(seqs_here, kv_count * group_size * head_width)


def shards(
    tokens,
    norm_gain,
    query_weight,
    key_weight,
    value_weight,
    forget_weight,
    forget_bias,
    kv_cache,
    log_gates,
    lengths,
    out_weight,
    mix_gain,
    expert_gate,
    expert_up,
    expert_down,
    routes,
    route_weights,
    dense_gate,
    dense_up,
    dense_down,
    gate_vector,
):
    seq_count = tokens.shape[0]
    normed = rms_scaled(tokens, norm_gain).astype(jnp.bfloat16)
    query_cols = query_weight.shape[1]
    key_cols = key_weight.shape[1]
    columns = lax.all_to_all(normed, "ep", split_axis=1, concat_axis=0, tiled=True)
    row_block = columns
    projected = lax.psum_scatter(
        jnp.concatenate(
            [
                jnp.dot(row_block, matrix, preferred_element_type=jnp.float32)
                for matrix in (query_weight, key_weight, value_weight, forget_weight)
            ],
            axis=1,
        ),
        "ep",
        scatter_dimension=0,
        tiled=True,
    )
    queries = projected[:, :query_cols].astype(jnp.bfloat16)
    key_new = projected[:, query_cols : query_cols + key_cols].astype(jnp.bfloat16)
    value_new = projected[:, query_cols + key_cols : query_cols + 2 * key_cols].astype(jnp.bfloat16)
    forget = jax.nn.log_sigmoid(projected[:, query_cols + 2 * key_cols :] + forget_bias)
    attended = attend_local(queries, key_new, value_new, forget, kv_cache, log_gates, lengths)
    column_terms = jnp.dot(
        lax.all_gather(attended, "ep", axis=0, tiled=True),
        out_weight,
        preferred_element_type=jnp.float32,
    )
    column_total = lax.psum(column_terms, "tp")
    summed = lax.all_to_all(column_total, "ep", split_axis=0, concat_axis=1, tiled=True)
    mixed = (tokens.astype(jnp.float32) + summed).astype(jnp.bfloat16)
    second = rms_scaled(mixed, mix_gain).astype(jnp.bfloat16)
    gate_value = jax.nn.sigmoid(
        jnp.dot(second.astype(jnp.float32), gate_vector, precision=lax.Precision.HIGHEST)
    )
    experts = lax.axis_size("ep")
    top_count = routes.shape[1]
    capacity = max(2, 2 * seq_count * top_count // experts)
    flat_routes = routes.reshape(-1)
    one_hot = (flat_routes[:, None] == jnp.arange(experts, dtype=jnp.int32)[None, :]).astype(
        jnp.int32
    )
    earlier = jnp.sum((jnp.cumsum(one_hot, axis=0) - one_hot) * one_hot, axis=1)
    slot_index = (flat_routes * capacity + earlier).reshape(seq_count, top_count)
    slot_ids = jnp.arange(experts * capacity, dtype=jnp.int32)
    dispatch_map = jnp.any(slot_index[None, :, :] == slot_ids[:, None, None], axis=2).astype(
        jnp.bfloat16
    )
    outgoing = jnp.dot(dispatch_map, second, preferred_element_type=jnp.float32).astype(
        jnp.bfloat16
    )
    outgoing = outgoing.reshape(experts, capacity, second.shape[1])
    received = lax.all_to_all(outgoing, "ep", split_axis=0, concat_axis=0, tiled=True)
    sources, items, model_width = received.shape
    flat_rows = received.reshape(sources * items, model_width)
    gate_pre = jnp.dot(flat_rows, expert_gate[0], preferred_element_type=jnp.float32)
    up_pre = jnp.dot(flat_rows, expert_up[0], preferred_element_type=jnp.float32)
    hidden = (jax.nn.silu(gate_pre) * up_pre).astype(jnp.bfloat16)
    partial_rows = jnp.dot(hidden, expert_down[0], preferred_element_type=jnp.float32)
    reduced = lax.psum_scatter(partial_rows, "tp", scatter_dimension=1, tiled=True)
    replies = reduced.astype(jnp.bfloat16).reshape(sources, items, reduced.shape[1])
    returned = lax.all_to_all(replies, "ep", split_axis=0, concat_axis=0, tiled=True)
    quarter_cols = returned.shape[2]
    picked = returned.reshape(experts * capacity, quarter_cols)[slot_index.reshape(-1)]
    routed = jnp.sum(
        picked.astype(jnp.float32).reshape(seq_count, top_count, quarter_cols)
        * route_weights[:, :, None],
        axis=1,
    )
    tp_index = lax.axis_index("tp")
    piece = lax.all_gather(second, "ep", axis=0, tiled=True)
    dense_hidden = (
        jax.nn.silu(jnp.dot(piece, dense_gate, preferred_element_type=jnp.float32))
        * jnp.dot(piece, dense_up, preferred_element_type=jnp.float32)
    ).astype(jnp.bfloat16)
    row_block = dense_hidden
    dense_out = lax.psum_scatter(
        jnp.dot(row_block, dense_down, preferred_element_type=jnp.float32),
        "ep",
        scatter_dimension=0,
        tiled=True,
    )
    residual = lax.dynamic_slice_in_dim(mixed, tp_index * quarter_cols, quarter_cols, 1).astype(
        jnp.float32
    )
    return (residual + routed + gate_value[:, None] * dense_out).astype(jnp.bfloat16)


def solution(mesh):
    return jax.shard_map(
        shards,
        mesh=mesh,
        in_specs=(
            P("ep", None),
            P(),
            P("ep", "tp"),
            P("ep", "tp"),
            P("ep", "tp"),
            P("ep", "tp"),
            P("tp"),
            P("ep", None, "tp", None),
            P("ep", None, "tp"),
            P("ep"),
            P("tp", "ep"),
            P(),
            P("ep", None, "tp"),
            P("ep", None, "tp"),
            P("ep", "tp", None),
            P("ep", None),
            P("ep", None),
            P(None, "ep"),
            P(None, "ep"),
            P("ep", "tp"),
            P(),
        ),
        out_specs=P("ep", "tp"),
        check_vma=False,
    )
```

profile of v0, /device:TPU:0, one launch (start us, length us, event | category | flops | bytes accessed | tf_op | source)
XLA Modules:
  0.0 333.0 jit_solution(12179301577359732236)
XLA Ops:
  6.6 1.2 fusion.48
  7.8 1.0 fusion.50
  8.9 14.4 %all_to_all.48 = bf16[16,8,512]{2,0,1:T(8,128)(2,1)S(1)} all-to-all(bf16[16,8,512]{2,0,1:T(8,128)(2,1)S(1)} %bitcast.121), channel_id=1, replica_groups=mesh['ep'=8,'tp'=4] {'ep'}, dimensions={1} | all-to-all | bytes 262144 | tf_op jit(solution)/shard_map/all_to_all | solution.py:84
  23.3 0.8 fusion.84
  24.1 1.0 fusion.83
  25.2 1.0 fusion.82
  26.2 1.3 fusion.81
  27.5 0.9 pad_maximum_fusion
  28.4 0.7 broadcast_add_fusion
  29.1 0.2 select_reduce_fusion
  29.4 59.1 %reduce-scatter.4.cloned.1.call-done = f32[16,648]{1,0:T(8,128)} async-done(((f32[128,648]{1,0:T(8,128)}), f32[16,648]{1,0:T(8,128)}) %reduce-scatter.4.cloned.1.call-update) | async-done | bytes 41488 | tf_op jit(solution)/shard_map/reduce_scatter | solution.py:86
  88.5 0.8 convert.6
  89.4 0.1 reshape.186
  89.5 0.1 fusion.71
  89.6 0.9 fusion.69
  90.5 3.7 %fusion.80 = (f32[16,8]{1,0:T(8,128)S(1)}, f32[16,1,8,1024]{3,2,0,1:T(8,128)S(1)}) fusion(f32[16,1024,8]{1,2,0:T(8,128)S(1)} %copy-done.3, f32[16,8]{1,0:T(8,128)S(1)} %fusion.69, bf16[16,8,64]{2,1,0:T(8,128)(2,1)S(1)} %reshape.186, bf16[16,1024,1,128]{3,1,2,0:T(8,128)(2,1)} %param.28, pred[16,1024]{1,0:T(8,128)(4,1)S(1)} %iota_compare_fusion.1), kind=kOutput, calls=%fused_computation.96 | convolution fusion | flops 17432448 | bytes 5276672 | tf_op jit(solution)/shard_map/skgd,slkd->skgl/dot_general | solution.py:31
  94.2 0.2 fusion.44
  94.5 1.4 fusion.37
  95.9 0.1 reshape.191
  96.0 30.5 %all_gather.6 = bf16[128,512]{1,0:T(8,128)(2,1)S(1)} all-gather(bf16[16,512]{1,0:T(8,128)(2,1)S(1)} %reshape.191), channel_id=1, replica_groups=mesh['ep'=8,'tp'=4] {'ep'}, dimensions={0}, use_global_device_ids=true | all-gather | bytes 147456 | tf_op jit(solution)/shard_map/all_gather | solution.py:104
  126.6 0.9 fusion.85
  127.7 31.3 %all-reduce.2.cloned.1.call-done = f32[8,16,512]{2,1,0:T(8,128)} async-done(((f32[8,16,512]{2,1,0:T(8,128)}), f32[8,16,512]{2,1,0:T(8,128)}) %all-reduce.2.cloned.1.call-update) | async-done | bytes 262160 | tf_op jit(solution)/shard_map/psum | solution.py:108
  159.0 5.5 %all-to-all-start.1 = ((f32[8,16,512]{2,1,0:T(8,128)}), f32[8,16,512]{2,1,0:T(8,128)S(1)}, u32[]{:S(2)}, u32[]{:S(2)}) async-start(f32[8,16,512]{2,1,0:T(8,128)} %all-reduce.2.cloned.1.call-done), calls=%async_computation.2 | async-start | bytes 524288 | tf_op jit(solution)/shard_map/all_to_all | solution.py:109
  164.6 0.1 reduce_window_sum.11
  164.7 0.2 select_reduce_fusion.1
  165.1 0.1 fusion.67
  165.2 7.6 %all-to-all-done.1 = f32[8,16,512]{2,1,0:T(8,128)S(1)} async-done(((f32[8,16,512]{2,1,0:T(8,128)}), f32[8,16,512]{2,1,0:T(8,128)S(1)}, u32[]{:S(2)}, u32[]{:S(2)}) %all-to-all-start.1) | async-done | bytes 262176 | tf_op jit(solution)/shard_map/all_to_all | solution.py:109
  172.8 0.2 fusion.45
  173.0 0.1 fusion.47
  173.1 1.5 convolution_convert_fusion
  174.6 3.6 %all-to-all-start.2 = ((bf16[8,16,4096]{2,1,0:T(8,128)(2,1)}), bf16[8,16,4096]{2,1,0:T(8,128)(2,1)S(1)}, u32[]{:S(2)}, u32[]{:S(2)}) async-start(bf16[8,16,4096]{2,1,0:T(8,128)(2,1)} %bitcast.112), calls=%async_computation.3 | async-start | bytes 2097152 | tf_op jit(solution)/shard_map/all_to_all | solution.py:132
  178.2 0.7 all-gather.2.cloned.1.call-update
  178.9 27.4 %all-to-all-done.2 = bf16[8,16,4096]{2,1,0:T(8,128)(2,1)S(1)} async-done(((bf16[8,16,4096]{2,1,0:T(8,128)(2,1)}), bf16[8,16,4096]{2,1,0:T(8,128)(2,1)S(1)}, u32[]{:S(2)}, u32[]{:S(2)}) %all-to-all-start.2) | async-done | bytes 1048608 | tf_op jit(solution)/shard_map/all_to_all | solution.py:132
  206.3 2.0 fusion.10
  208.4 4.3 %fusion.6 = f32[128,4096]{1,0:T(8,128)} fusion(bf16[1,256,4096]{2,1,0:T(8,128)(2,1)S(1)} %copy-done, bf16[128,4096]{1,0:T(8,128)(2,1)S(1)} %bitcast.110, bf16[1,4096,256]{2,1,0:T(8,128)(2,1)} %param.34, f32[128,256]{1,0:T(8,128)S(1)} %fusion.10), kind=kOutput, calls=%fused_computation.8 | convolution fusion | flops 537067520 | bytes 7471104 | tf_op jit(solution)/shard_map/dot_general | solution.py:138
  212.7 14.0 %all-gather.2.cloned.1.call-done = bf16[128,4096]{1,0:T(8,128)(2,1)} async-done(((bf16[16,4096]{1,0:T(8,128)(2,1)}), bf16[128,4096]{1,0:T(8,128)(2,1)}) %all-gather.2.cloned.1.call-update) | async-done | bytes 1048592 | tf_op jit(solution)/shard_map/all_gather | solution.py:150
  226.7 3.3 fusion.86
  230.1 4.3 %fusion.25 = f32[128,1024]{1,0:T(8,128)} fusion(bf16[512,1024]{1,0:T(8,128)(2,1)} %param.40, bf16[128,4096]{1,0:T(8,128)(2,1)S(1)} %copy-done.2, bf16[4096,512]{1,0:T(8,128)(2,1)} %param.39, f32[128,512]{1,0:T(8,128)S(1)} %fusion.86), kind=kOutput, calls=%fused_computation.20 | convolution fusion | flops 671481856 | bytes 7077888 | tf_op jit(solution)/shard_map/dot_general | solution.py:157
  234.6 24.5 %reduce-scatter.6.cloned.1.call-done = f32[128,1024]{1,0:T(8,128)} async-done(((f32[128,4096]{1,0:T(8,128)}), f32[128,1024]{1,0:T(8,128)}) %reduce-scatter.6.cloned.1.call-update) | async-done | bytes 524304 | tf_op jit(solution)/shard_map/reduce_scatter | solution.py:139
  259.0 1.8 convert_element_type.82
  260.8 5.5 %all-to-all-start.3 = ((bf16[8,16,1024]{2,1,0:T(8,128)(2,1)}), bf16[8,16,1024]{2,1,0:T(8,128)(2,1)S(1)}, u32[]{:S(2)}, u32[]{:S(2)}) async-start(bf16[8,16,1024]{2,1,0:T(8,128)(2,1)} %bitcast.19), calls=%async_computation.5 | async-start | bytes 524288 | tf_op jit(solution)/shard_map/all_to_all | solution.py:141
  266.4 0.9 fusion.43
  267.3 8.6 %all-to-all-done.3 = bf16[8,16,1024]{2,1,0:T(8,128)(2,1)S(1)} async-done(((bf16[8,16,1024]{2,1,0:T(8,128)(2,1)}), bf16[8,16,1024]{2,1,0:T(8,128)(2,1)S(1)}, u32[]{:S(2)}, u32[]{:S(2)}) %all-to-all-start.3) | async-done | bytes 262176 | tf_op jit(solution)/shard_map/all_to_all | solution.py:141
  275.9 0.7 gather_fusion
  276.6 0.1 reshape.196
  276.7 0.2 multiply_reduce_fusion
  276.9 48.0 %reduce-scatter.8.cloned.1.call-done = f32[16,1024]{1,0:T(8,128)} async-done(((f32[128,1024]{1,0:T(8,128)}), f32[16,1024]{1,0:T(8,128)}) %reduce-scatter.8.cloned.1.call-update) | async-done | bytes 65552 | tf_op jit(solution)/shard_map/reduce_scatter | solution.py:156
  324.9 1.5 add_convert_fusion
  (57 shorter events, 1.2 us)
Async XLA Ops:
  6.5 201.8 %copy-start = (bf16[1,256,4096]{2,1,0:T(8,128)(2,1)S(1)}, bf16[1,256,4096]{2,1,0:T(8,128)(2,1)}, u32[]{:S(2)}) copy-start(bf16[1,256,4096]{2,1,0:T(8,128)(2,1)} %param.35) | copy-start | bytes 6291460
  6.5 22.8 %copy-start.12 = (s32[16]{0:T(128)S(1)}, s32[16]{0:T(128)}, u32[]{:S(2)}) copy-start(s32[16]{0:T(128)} %param.30) | copy-start | bytes 196
  6.5 22.6 %copy-start.3 = (f32[16,1024,8]{1,2,0:T(8,128)S(1)}, f32[16,1024,8]{1,2,0:T(8,128)}, u32[]{:S(2)}) copy-start(f32[16,1024,8]{1,2,0:T(8,128)} %param.29) | copy-start | bytes 1572868
  6.5 83.1 %copy-start.13 = (f32[8]{0:T(128)S(1)}, f32[8]{0:T(128)}, u32[]{:S(2)}) copy-start(f32[8]{0:T(128)} %param.27) | copy-start | bytes 100
  6.5 82.0 %reduce-scatter.4.cloned.1.call-start = ((), (), s32[]{:S(2)}) async-start(), calls=%async_computation.7 | async-start | bytes 442368 | tf_op jit(solution)/shard_map/reduce_scatter | solution.py:86
  28.3 130.7 %all-reduce.2.cloned.1.call-start = ((), (), s32[]{:S(2)}) async-start(), calls=%async_computation.8 | async-start | bytes 524288 | tf_op jit(solution)/shard_map/psum | solution.py:108
  89.5 5.0 %copy-start.1 = (bf16[16,1024,1,128]{3,1,2,0:T(8,128)(2,1)S(1)}, bf16[16,1024,1,128]{3,1,2,0:T(8,128)(2,1)}, u32[]{:S(2)}) copy-start(bf16[16,1024,1,128]{3,1,2,0:T(8,128)(2,1)} %param.28) | copy-start | bytes 12582916
  94.2 32.3 %copy-start.8 = (bf16[512,512]{1,0:T(8,128)(2,1)S(1)}, bf16[512,512]{1,0:T(8,128)(2,1)}, u32[]{:S(2)}) copy-start(bf16[512,512]{1,0:T(8,128)(2,1)} %param.31) | copy-start | bytes 1572868
  94.2 33.3 %copy-start.10 = (s32[16,4]{0,1:T(4,128)S(1)}, s32[16,4]{0,1:T(4,128)}, u32[]{:S(2)}) copy-start(s32[16,4]{0,1:T(4,128)} %param.36) | copy-start | bytes 772
  94.5 78.3 %copy-start.4 = (bf16[16,4096]{1,0:T(8,128)(2,1)S(1)}, bf16[16,4096]{1,0:T(8,128)(2,1)}, u32[]{:S(2)}) copy-start(bf16[16,4096]{1,0:T(8,128)(2,1)} %param.21) | copy-start | bytes 393220
  94.5 78.5 %copy-start.9 = (f32[4096]{0:T(1024)S(1)}, f32[4096]{0:T(1024)}, u32[]{:S(2)}) copy-start(f32[4096]{0:T(1024)} %param.32) | copy-start | bytes 49156
  159.0 13.7 %all-to-all-start.1 = ((f32[8,16,512]{2,1,0:T(8,128)}), f32[8,16,512]{2,1,0:T(8,128)S(1)}, u32[]{:S(2)}, u32[]{:S(2)}) async-start(f32[8,16,512]{2,1,0:T(8,128)} %all-reduce.2.cloned.1.call-done), calls=%async_computation.2 | async-start | bytes 524288 | tf_op jit(solution)/shard_map/all_to_all | solution.py:109
  173.0 1.6 copy-start.7
  173.1 5.1 %copy-start.5 = (bf16[16,4096]{1,0:T(8,128)(2,1)}, bf16[16,4096]{1,0:T(8,128)(2,1)S(1)}, u32[]{:S(2)}) copy-start(bf16[16,4096]{1,0:T(8,128)(2,1)S(1)} %fusion.47) | copy-start | bytes 393220
  174.6 31.8 %all-to-all-start.2 = ((bf16[8,16,4096]{2,1,0:T(8,128)(2,1)}), bf16[8,16,4096]{2,1,0:T(8,128)(2,1)S(1)}, u32[]{:S(2)}, u32[]{:S(2)}) async-start(bf16[8,16,4096]{2,1,0:T(8,128)(2,1)} %bitcast.112), calls=%async_computation.3 | async-start | bytes 2097152 | tf_op jit(solution)/shard_map/all_to_all | solution.py:132
  178.1 48.6 %all-gather.2.cloned.1.call-start = ((), (), s32[]{:S(2)}) async-start(), calls=%async_computation.10 | async-start | bytes 1179648 | tf_op jit(solution)/shard_map/all_gather | solution.py:150
  178.9 80.2 %reduce-scatter.6.cloned.1.call-start = ((), (), s32[]{:S(2)}) async-start(), calls=%async_computation.9 | async-start | bytes 2621440 | tf_op jit(solution)/shard_map/reduce_scatter | solution.py:139
  212.7 112.2 %reduce-scatter.8.cloned.1.call-start = ((), (), s32[]{:S(2)}) async-start(), calls=%async_computation.11 | async-start | bytes 589824 | tf_op jit(solution)/shard_map/reduce_scatter | solution.py:156
  226.7 3.3 copy-start.2
  230.1 4.3 %copy-start.11 = (f32[16,4]{0,1:T(4,128)S(1)}, f32[16,4]{0,1:T(4,128)}, u32[]{:S(2)}) copy-start(f32[16,4]{0,1:T(4,128)} %param.37) | copy-start | bytes 772
  230.1 36.3 %copy-start.6 = (bf16[16,4096]{1,0:T(8,128)(2,1)S(1)}, bf16[16,4096]{1,0:T(8,128)(2,1)}, u32[]{:S(2)}) copy-start(bf16[16,4096]{1,0:T(8,128)(2,1)} %copy-done.5) | copy-start | bytes 393220
  260.8 15.1 %all-to-all-start.3 = ((bf16[8,16,1024]{2,1,0:T(8,128)(2,1)}), bf16[8,16,1024]{2,1,0:T(8,128)(2,1)S(1)}, u32[]{:S(2)}, u32[]{:S(2)}) async-start(bf16[8,16,1024]{2,1,0:T(8,128)(2,1)} %bitcast.19), calls=%async_computation.5 | async-start | bytes 524288 | tf_op jit(solution)/shard_map/all_to_all | solution.py:141
Sparse Core Ops, SparseCore 0:
  28.5 60.0 reduce-scatter.3
  127.6 31.3 all-reduce.1
  181.1 45.6 all-gather.1
  229.1 29.8 reduce-scatter.5
  262.2 62.6 reduce-scatter.7
where the time goes:
time: 334 us; the launch traced here: 333 us
  waiting for transfers between devices  221 us (66%)
  blocking collectives  44.9 us (13%)
  matrix products  26.6 us (8%)
  starting transfers between devices  14.8 us (4%)
  between operations  13.5 us (4%)
  other arithmetic  10.4 us (3%)
    reduce_scatter x1, waiting for transfers between devices, shards(): lax.psum_scatter(jnp.concatenate([jnp.dot(row_block, matrix, preferred_el...  59.1 us
    reduce_scatter x1, waiting for transfers between devices, shards(): lax.psum_scatter(jnp.dot(row_block, dense_down, preferred_element_type=jn...  48 us
    psum x1, waiting for transfers between devices, shards(): column_total = lax.psum(column_terms, 'tp')  31.3 us
    all_gather x1, blocking collectives, shards(): lax.all_gather(attended, 'ep', axis=0, tiled=True)  30.5 us
    all_to_all x1, waiting for transfers between devices, shards(): lax.all_to_all(outgoing, 'ep', split_axis=0, concat_axis=0, tiled=True)  27.4 us
    reduce_scatter x1, waiting for transfers between devices, shards(): lax.psum_scatter(partial_rows, 'tp', scatter_dimension=1, tiled=True)  24.5 us
    all_to_all x1, blocking collectives, shards(): lax.all_to_all(normed, 'ep', split_axis=1, concat_axis=0, tiled=True)  14.4 us
    all_gather x1, waiting for transfers between devices, shards(): piece = lax.all_gather(second, 'ep', axis=0, tiled=True)  14 us
  transfers between devices with their start and end apart: 8, of which 8 were waited for; matrix products, arithmetic and copies ran while one was open for 6% of the time, Pallas kernels for 0%

commit v1 on v0

--- a/solution.py
+++ b/solution.py
@@ -105,7 +105,8 @@
         out_weight,
         preferred_element_type=jnp.float32,
     )
-    column_total = lax.psum(column_terms, "tp")
+    pieces = lax.all_gather(column_terms, "tp", axis=0, tiled=False)
+    column_total = pieces.sum(axis=0)
     summed = lax.all_to_all(column_total, "ep", split_axis=0, concat_axis=1, tiled=True)
     mixed = (tokens.astype(jnp.float32) + summed).astype(jnp.bfloat16)
     second = rms_scaled(mixed, mix_gain).astype(jnp.bfloat16)

time: 334 us -> 322 us (0.964)
  waiting for transfers between devices: 221 us -> 207 us
    psum x1 -> x0, waiting for transfers between devices: 31.3 us -> none  [shards(): column_total = lax.psum(column_terms, 'tp')]
    all_gather x0 -> x1, waiting for transfers between devices: none -> 15.7 us  [shards(): pieces = lax.all_gather(column_terms, 'tp', axis=0, tiled=False)]
where the time goes in v1:
time: 322 us; the launch traced here: 321 us
  waiting for transfers between devices  207 us (64%)
  blocking collectives  44.9 us (14%)
  matrix products  26.6 us (8%)
  starting transfers between devices  14.8 us (5%)
  between operations  13.4 us (4%)
  other arithmetic  12.4 us (4%)
    reduce_scatter x1, waiting for transfers between devices, shards(): lax.psum_scatter(jnp.concatenate([jnp.dot(row_block, matrix, preferred_el...  59.1 us
    reduce_scatter x1, waiting for transfers between devices, shards(): lax.psum_scatter(jnp.dot(row_block, dense_down, preferred_element_type=jn...  48 us
    all_gather x1, blocking collectives, shards(): lax.all_gather(attended, 'ep', axis=0, tiled=True)  30.5 us
    all_to_all x1, waiting for transfers between devices, shards(): lax.all_to_all(outgoing, 'ep', split_axis=0, concat_axis=0, tiled=True)  29.2 us
    reduce_scatter x1, waiting for transfers between devices, shards(): lax.psum_scatter(partial_rows, 'tp', scatter_dimension=1, tiled=True)  24.5 us
    all_gather x1, waiting for transfers between devices, shards(): pieces = lax.all_gather(column_terms, 'tp', axis=0, tiled=False)  15.7 us
    all_to_all x1, blocking collectives, shards(): lax.all_to_all(normed, 'ep', split_axis=1, concat_axis=0, tiled=True)  14.4 us
    all_gather x1, waiting for transfers between devices, shards(): piece = lax.all_gather(second, 'ep', axis=0, tiled=True)  12.6 us
  transfers between devices with their start and end apart: 8, of which 8 were waited for; matrix products, arithmetic and copies ran while one was open for 6% of the time, Pallas kernels for 0%

profile of v1, /device:TPU:0, one launch (start us, length us, event | category | flops | bytes accessed | tf_op | source)
XLA Modules:
  0.0 320.9 jit_solution(13253524367830139938)
XLA Ops:
  6.6 1.2 fusion.48
  7.8 1.0 fusion.50
  8.9 14.4 %all_to_all.48 = bf16[16,8,512]{2,0,1:T(8,128)(2,1)S(1)} all-to-all(bf16[16,8,512]{2,0,1:T(8,128)(2,1)S(1)} %bitcast.122), channel_id=1, replica_groups=mesh['ep'=8,'tp'=4] {'ep'}, dimensions={1} | all-to-all | bytes 262144 | tf_op jit(solution)/shard_map/all_to_all | solution.py:84
  23.3 0.8 fusion.84
  24.1 1.0 fusion.83
  25.2 1.0 fusion.82
  26.2 1.3 fusion.81
  27.5 0.9 pad_maximum_fusion
  28.4 0.7 broadcast_add_fusion
  29.1 0.2 select_reduce_fusion
  29.4 59.1 %reduce-scatter.4.cloned.1.call-done = f32[16,648]{1,0:T(8,128)} async-done(((f32[128,648]{1,0:T(8,128)}), f32[16,648]{1,0:T(8,128)}) %reduce-scatter.4.cloned.1.call-update) | async-done | bytes 41488 | tf_op jit(solution)/shard_map/reduce_scatter | solution.py:86
  88.5 0.8 convert.6
  89.4 0.1 reshape.186
  89.5 0.1 fusion.71
  89.6 0.9 fusion.69
  90.5 3.7 %fusion.80 = (f32[16,8]{1,0:T(8,128)S(1)}, f32[16,1,8,1024]{3,2,0,1:T(8,128)S(1)}) fusion(f32[16,1024,8]{1,2,0:T(8,128)S(1)} %copy-done.3, f32[16,8]{1,0:T(8,128)S(1)} %fusion.69, bf16[16,8,64]{2,1,0:T(8,128)(2,1)S(1)} %reshape.186, bf16[16,1024,1,128]{3,1,2,0:T(8,128)(2,1)} %param.28, pred[16,1024]{1,0:T(8,128)(4,1)S(1)} %iota_compare_fusion.1), kind=kOutput, calls=%fused_computation.96 | convolution fusion | flops 17432448 | bytes 5276672 | tf_op jit(solution)/shard_map/skgd,slkd->skgl/dot_general | solution.py:31
  94.2 0.2 fusion.44
  94.5 1.4 fusion.37
  95.9 0.1 reshape.191
  96.0 30.5 %all_gather.12 = bf16[128,512]{1,0:T(8,128)(2,1)S(1)} all-gather(bf16[16,512]{1,0:T(8,128)(2,1)S(1)} %reshape.191), channel_id=1, replica_groups=mesh['ep'=8,'tp'=4] {'ep'}, dimensions={0}, use_global_device_ids=true | all-gather | bytes 147456 | tf_op jit(solution)/shard_map/all_gather | solution.py:104
  126.6 1.0 fusion.85
  127.7 15.7 %all-gather.6.cloned.1.call-done = f32[512,512]{1,0:T(8,128)} async-done(((f32[128,512]{1,0:T(8,128)}), f32[512,512]{1,0:T(8,128)}) %all-gather.6.cloned.1.call-update) | async-done | bytes 1048592 | tf_op jit(solution)/shard_map/all_gather | solution.py:108
  143.4 2.0 reduce_sum.70
  145.5 5.5 %all-to-all-start.1 = ((f32[8,16,512]{2,1,0:T(8,128)}), f32[8,16,512]{2,1,0:T(8,128)S(1)}, u32[]{:S(2)}, u32[]{:S(2)}) async-start(f32[8,16,512]{2,1,0:T(8,128)} %bitcast.13), calls=%async_computation.2 | async-start | bytes 524288 | tf_op jit(solution)/shard_map/all_to_all | solution.py:110
  151.1 0.1 reduce_window_sum.11
  151.2 0.2 select_reduce_fusion.1
  151.6 8.7 %all-to-all-done.1 = f32[8,16,512]{2,1,0:T(8,128)S(1)} async-done(((f32[8,16,512]{2,1,0:T(8,128)}), f32[8,16,512]{2,1,0:T(8,128)S(1)}, u32[]{:S(2)}, u32[]{:S(2)}) %all-to-all-start.1) | async-done | bytes 262176 | tf_op jit(solution)/shard_map/all_to_all | solution.py:110
  160.3 0.2 fusion.45
  160.5 0.1 fusion.47
  160.7 1.5 convolution_convert_fusion
  162.1 3.6 %all-to-all-start.2 = ((bf16[8,16,4096]{2,1,0:T(8,128)(2,1)}), bf16[8,16,4096]{2,1,0:T(8,128)(2,1)S(1)}, u32[]{:S(2)}, u32[]{:S(2)}) async-start(bf16[8,16,4096]{2,1,0:T(8,128)(2,1)} %bitcast.113), calls=%async_computation.3 | async-start | bytes 2097152 | tf_op jit(solution)/shard_map/all_to_all | solution.py:133
  165.7 0.7 all-gather.4.cloned.1.call-update
  166.5 29.2 %all-to-all-done.2 = bf16[8,16,4096]{2,1,0:T(8,128)(2,1)S(1)} async-done(((bf16[8,16,4096]{2,1,0:T(8,128)(2,1)}), bf16[8,16,4096]{2,1,0:T(8,128)(2,1)S(1)}, u32[]{:S(2)}, u32[]{:S(2)}) %all-to-all-start.2) | async-done | bytes 1048608 | tf_op jit(solution)/shard_map/all_to_all | solution.py:133
  195.6 2.0 fusion.10
  197.7 4.3 %fusion.6 = f32[128,4096]{1,0:T(8,128)} fusion(bf16[1,256,4096]{2,1,0:T(8,128)(2,1)S(1)} %copy-done, bf16[128,4096]{1,0:T(8,128)(2,1)S(1)} %bitcast.111, bf16[1,4096,256]{2,1,0:T(8,128)(2,1)} %param.34, f32[128,256]{1,0:T(8,128)S(1)} %fusion.10), kind=kOutput, calls=%fused_computation.8 | convolution fusion | flops 537067520 | bytes 7471104 | tf_op jit(solution)/shard_map/dot_general | solution.py:139
  202.0 12.6 %all-gather.4.cloned.1.call-done = bf16[128,4096]{1,0:T(8,128)(2,1)} async-done(((bf16[16,4096]{1,0:T(8,128)(2,1)}), bf16[128,4096]{1,0:T(8,128)(2,1)}) %all-gather.4.cloned.1.call-update) | async-done | bytes 1048592 | tf_op jit(solution)/shard_map/all_gather | solution.py:151
  214.7 3.3 %fusion.86 = f32[128,512]{1,0:T(8,128)S(1)} fusion(bf16[128,4096]{1,0:T(8,128)(2,1)} %all-gather.4.cloned.1.call-done, bf16[4096,512]{1,0:T(8,128)(2,1)} %param.38), kind=kOutput, calls=%fused_computation.102 | convolution fusion | flops 536870912 | bytes 5505024 | tf_op jit(solution)/shard_map/dot_general | solution.py:153
  218.0 4.3 %fusion.25 = f32[128,1024]{1,0:T(8,128)} fusion(bf16[512,1024]{1,0:T(8,128)(2,1)} %param.40, bf16[128,4096]{1,0:T(8,128)(2,1)S(1)} %copy-done.2, bf16[4096,512]{1,0:T(8,128)(2,1)} %param.39, f32[128,512]{1,0:T(8,128)S(1)} %fusion.86), kind=kOutput, calls=%fused_computation.20 | convolution fusion | flops 671481856 | bytes 7077888 | tf_op jit(solution)/shard_map/dot_general | solution.py:158
  222.5 24.5 %reduce-scatter.6.cloned.1.call-done = f32[128,1024]{1,0:T(8,128)} async-done(((f32[128,4096]{1,0:T(8,128)}), f32[128,1024]{1,0:T(8,128)}) %reduce-scatter.6.cloned.1.call-update) | async-done | bytes 524304 | tf_op jit(solution)/shard_map/reduce_scatter | solution.py:140
  247.0 1.8 convert_element_type.82
  248.8 5.5 %all-to-all-start.3 = ((bf16[8,16,1024]{2,1,0:T(8,128)(2,1)}), bf16[8,16,1024]{2,1,0:T(8,128)(2,1)S(1)}, u32[]{:S(2)}, u32[]{:S(2)}) async-start(bf16[8,16,1024]{2,1,0:T(8,128)(2,1)} %bitcast.20), calls=%async_computation.5 | async-start | bytes 524288 | tf_op jit(solution)/shard_map/all_to_all | solution.py:142
  254.3 0.9 fusion.43
  255.2 8.6 %all-to-all-done.3 = bf16[8,16,1024]{2,1,0:T(8,128)(2,1)S(1)} async-done(((bf16[8,16,1024]{2,1,0:T(8,128)(2,1)}), bf16[8,16,1024]{2,1,0:T(8,128)(2,1)S(1)}, u32[]{:S(2)}, u32[]{:S(2)}) %all-to-all-start.3) | async-done | bytes 262176 | tf_op jit(solution)/shard_map/all_to_all | solution.py:142
  263.8 0.7 gather_fusion
  264.5 0.1 reshape.196
  264.6 0.2 multiply_reduce_fusion
  264.9 48.0 %reduce-scatter.8.cloned.1.call-done = f32[16,1024]{1,0:T(8,128)} async-done(((f32[128,1024]{1,0:T(8,128)}), f32[16,1024]{1,0:T(8,128)}) %reduce-scatter.8.cloned.1.call-update) | async-done | bytes 65552 | tf_op jit(solution)/shard_map/reduce_scatter | solution.py:157
  312.8 1.5 add_convert_fusion
  (58 shorter events, 1.3 us)
Async XLA Ops:
  6.5 191.2 %copy-start = (bf16[1,256,4096]{2,1,0:T(8,128)(2,1)S(1)}, bf16[1,256,4096]{2,1,0:T(8,128)(2,1)}, u32[]{:S(2)}) copy-start(bf16[1,256,4096]{2,1,0:T(8,128)(2,1)} %param.35) | copy-start | bytes 6291460
  6.5 22.8 %copy-start.12 = (s32[16]{0:T(128)S(1)}, s32[16]{0:T(128)}, u32[]{:S(2)}) copy-start(s32[16]{0:T(128)} %param.30) | copy-start | bytes 196
  6.5 22.6 %copy-start.3 = (f32[16,1024,8]{1,2,0:T(8,128)S(1)}, f32[16,1024,8]{1,2,0:T(8,128)}, u32[]{:S(2)}) copy-start(f32[16,1024,8]{1,2,0:T(8,128)} %param.29) | copy-start | bytes 1572868
  6.5 83.1 %copy-start.13 = (f32[8]{0:T(128)S(1)}, f32[8]{0:T(128)}, u32[]{:S(2)}) copy-start(f32[8]{0:T(128)} %param.27) | copy-start | bytes 100
  6.5 82.0 %reduce-scatter.4.cloned.1.call-start = ((), (), s32[]{:S(2)}) async-start(), calls=%async_computation.7 | async-start | bytes 442368 | tf_op jit(solution)/shard_map/reduce_scatter | solution.py:86
  28.3 115.1 %all-gather.6.cloned.1.call-start = ((), (), s32[]{:S(2)}) async-start(), calls=%async_computation.11 | async-start | bytes 1310720 | tf_op jit(solution)/shard_map/all_gather | solution.py:108
  89.5 5.0 %copy-start.1 = (bf16[16,1024,1,128]{3,1,2,0:T(8,128)(2,1)S(1)}, bf16[16,1024,1,128]{3,1,2,0:T(8,128)(2,1)}, u32[]{:S(2)}) copy-start(bf16[16,1024,1,128]{3,1,2,0:T(8,128)(2,1)} %param.28) | copy-start | bytes 12582916
  94.2 32.3 %copy-start.8 = (bf16[512,512]{1,0:T(8,128)(2,1)S(1)}, bf16[512,512]{1,0:T(8,128)(2,1)}, u32[]{:S(2)}) copy-start(bf16[512,512]{1,0:T(8,128)(2,1)} %param.31) | copy-start | bytes 1572868
  94.2 33.3 %copy-start.10 = (s32[16,4]{0,1:T(4,128)S(1)}, s32[16,4]{0,1:T(4,128)}, u32[]{:S(2)}) copy-start(s32[16,4]{0,1:T(4,128)} %param.36) | copy-start | bytes 772
  94.5 65.8 %copy-start.4 = (bf16[16,4096]{1,0:T(8,128)(2,1)S(1)}, bf16[16,4096]{1,0:T(8,128)(2,1)}, u32[]{:S(2)}) copy-start(bf16[16,4096]{1,0:T(8,128)(2,1)} %param.21) | copy-start | bytes 393220
  94.5 66.0 %copy-start.9 = (f32[4096]{0:T(1024)S(1)}, f32[4096]{0:T(1024)}, u32[]{:S(2)}) copy-start(f32[4096]{0:T(1024)} %param.32) | copy-start | bytes 49156
  145.5 14.8 %all-to-all-start.1 = ((f32[8,16,512]{2,1,0:T(8,128)}), f32[8,16,512]{2,1,0:T(8,128)S(1)}, u32[]{:S(2)}, u32[]{:S(2)}) async-start(f32[8,16,512]{2,1,0:T(8,128)} %bitcast.13), calls=%async_computation.2 | async-start | bytes 524288 | tf_op jit(solution)/shard_map/all_to_all | solution.py:110
  160.5 1.6 copy-start.7
  160.6 5.1 %copy-start.5 = (bf16[16,4096]{1,0:T(8,128)(2,1)}, bf16[16,4096]{1,0:T(8,128)(2,1)S(1)}, u32[]{:S(2)}) copy-start(bf16[16,4096]{1,0:T(8,128)(2,1)S(1)} %fusion.47) | copy-start | bytes 393220
  162.1 33.5 %all-to-all-start.2 = ((bf16[8,16,4096]{2,1,0:T(8,128)(2,1)}), bf16[8,16,4096]{2,1,0:T(8,128)(2,1)S(1)}, u32[]{:S(2)}, u32[]{:S(2)}) async-start(bf16[8,16,4096]{2,1,0:T(8,128)(2,1)} %bitcast.113), calls=%async_computation.3 | async-start | bytes 2097152 | tf_op jit(solution)/shard_map/all_to_all | solution.py:133
  165.7 49.0 %all-gather.4.cloned.1.call-start = ((), (), s32[]{:S(2)}) async-start(), calls=%async_computation.9 | async-start | bytes 1179648 | tf_op jit(solution)/shard_map/all_gather | solution.py:151
  166.4 80.5 %reduce-scatter.6.cloned.1.call-start = ((), (), s32[]{:S(2)}) async-start(), calls=%async_computation.8 | async-start | bytes 2621440 | tf_op jit(solution)/shard_map/reduce_scatter | solution.py:140
  202.0 110.9 %reduce-scatter.8.cloned.1.call-start = ((), (), s32[]{:S(2)}) async-start(), calls=%async_computation.10 | async-start | bytes 589824 | tf_op jit(solution)/shard_map/reduce_scatter | solution.py:157
  214.7 3.3 %copy-start.2 = (bf16[128,4096]{1,0:T(8,128)(2,1)S(1)}, bf16[128,4096]{1,0:T(8,128)(2,1)}, u32[]{:S(2)}) copy-start(bf16[128,4096]{1,0:T(8,128)(2,1)} %all-gather.4.cloned.1.call-done) | copy-start | bytes 3145732
  218.0 4.3 %copy-start.11 = (f32[16,4]{0,1:T(4,128)S(1)}, f32[16,4]{0,1:T(4,128)}, u32[]{:S(2)}) copy-start(f32[16,4]{0,1:T(4,128)} %param.37) | copy-start | bytes 772
  218.0 36.3 %copy-start.6 = (bf16[16,4096]{1,0:T(8,128)(2,1)S(1)}, bf16[16,4096]{1,0:T(8,128)(2,1)}, u32[]{:S(2)}) copy-start(bf16[16,4096]{1,0:T(8,128)(2,1)} %copy-done.5) | copy-start | bytes 393220
  248.8 15.1 %all-to-all-start.3 = ((bf16[8,16,1024]{2,1,0:T(8,128)(2,1)}), bf16[8,16,1024]{2,1,0:T(8,128)(2,1)S(1)}, u32[]{:S(2)}, u32[]{:S(2)}) async-start(bf16[8,16,1024]{2,1,0:T(8,128)(2,1)} %bitcast.20), calls=%async_computation.5 | async-start | bytes 524288 | tf_op jit(solution)/shard_map/all_to_all | solution.py:142
Sparse Core Ops, SparseCore 0:
  28.5 60.0 reduce-scatter.3
  127.7 15.7 all-gather.5
  168.6 45.9 all-gather.3
  217.0 29.8 reduce-scatter.5
  250.2 62.6 reduce-scatter.7
